TPU v7x, 32 devices: a whole 2x2x4 slice. The times are simulated.
32 devices in a mesh: fs: 16 (over z, y, x), tp: 2 (over core).
Axes of the slice: x: 2, y: 2, z: 4, core: 2. Of those that a mesh axis runs over, the one named last changes fastest.
Arguments:
- tokens: bfloat16 [4096, 2048], P('fs'), may hold values from -6 to 6
- routes: int32 [4096, 6], P('fs'), may hold values from 0 to 15, all different within a row; in each aligned block of 256 rows (0 to 255, 256 to 511, ...) at most 160 rows name the same one
- route_weights: float32 [4096, 6], P('fs'), may hold values from 0.1 to 1
- norm_gain: float32 [2048], P('fs'), may hold values from 0.1 to 1.9
- expert_gate: float32 [16, 2048, 1024], P(None, 'fs', 'tp'), may hold values from -0.125 to 0.125
- expert_up: float32 [16, 2048, 1024], P(None, 'fs', 'tp'), may hold values from -0.125 to 0.125
- expert_down: float32 [16, 2048, 1024], P(None, 'fs', 'tp'), may hold values from -0.1875 to 0.1875
- shared_gate: float32 [2048, 1024], P('fs', 'tp'), may hold values from -0.125 to 0.125
- shared_up: float32 [2048, 1024], P('fs', 'tp'), may hold values from -0.125 to 0.125
- shared_down: float32 [2048, 1024], P('fs', 'tp'), may hold values from -0.1875 to 0.1875
Outputs:
- layer_output: bfloat16 [4096, 2048], P('fs', 'tp')
- sample_gate: bfloat16 [16, 2048, 1024], P('fs', None, 'tp')
- sample_up: bfloat16 [16, 2048, 1024], P('fs', None, 'tp')
- sample_down: bfloat16 [16, 2048, 1024], P('fs', None, 'tp')
- common_gate: bfloat16 [2048, 1024], P(None, 'tp')
- common_up: bfloat16 [2048, 1024], P(None, 'tp')
- common_down: bfloat16 [2048, 1024], P(None, 'tp')
Inputs may be any that keep to these rules, and one draw needn't show every extreme that they name: `routes`: each row names 6 different experts. In each aligned block of 256 rows (the rows of one index of fs) no expert is named by more than 160 rows, a bound that some expert reaches in some blocks.
All inputs are finite; a program needn't handle non-finite values.
Results may differ from a plain program's by a relative error of at most 0.015.
Values may be sent and summed in bfloat16 or wider, within the bound.
A program may use at most 128 MiB of HBM per device.

v0:
```python
import jax
import jax.numpy as jnp
from jax import lax
from jax.sharding import PartitionSpec as P

EPSILON = 1e-06


def normalize(tokens):
    values = tokens.astype(jnp.float32)
    scale = lax.rsqrt(jnp.mean(values * values, axis=-1, keepdims=True) + EPSILON)
    return (values * scale).astype(jnp.bfloat16)


def ring_of(fs_count):
    if fs_count != 16:
        return list(range(fs_count))
    order = []
    for place, column in enumerate((0, 1, 3, 2)):
        heights = range(4) if place % 2 == 0 else range(3, -1, -1)
        order.extend((height * 4 + column for height in heights))
    return order


def reorder(blocks, order):
    if list(order) == list(range(len(order))):
        return blocks
    return jnp.concatenate([blocks[i : i + 1] for i in order], axis=0)


def body(
    tokens,
    routes,
    route_weights,
    norm_gain,
    expert_gate,
    expert_up,
    expert_down,
    shared_gate,
    shared_up,
    shared_down,
):
    tp_count = lax.axis_size("tp")
    tp_index = lax.axis_index("tp")
    fs_count = lax.axis_size("fs")
    tok_rows, width = tokens.shape
    experts = expert_gate.shape[0]
    share = tok_rows // tp_count
    own_experts = experts // fs_count
    ring = ring_of(fs_count)
    place_of = [ring.index(i) for i in range(fs_count)]
    groups = None if ring == list(range(fs_count)) else [ring]
    normed = normalize(tokens)
    own_normed = lax.dynamic_slice_in_dim(normed, tp_index * share, share, 0)
    own_routes = lax.dynamic_slice_in_dim(routes, tp_index * share, share, 0)
    own_weights = lax.dynamic_slice_in_dim(route_weights, tp_index * share, share, 0)
    member = own_routes[None, :, :] == jnp.arange(experts, dtype=jnp.int32)[:, None, None]
    dense = jnp.sum(jnp.where(member, own_weights[None, :, :], 0.0), axis=2)
    dense_all = lax.all_gather(dense, "fs", axis=0, tiled=False)
    own_normed, dense_all = lax.optimization_barrier((own_normed, dense_all))
    gathered = lax.all_gather(own_normed, "fs", axis=0, tiled=False)
    gathered = reorder(gathered, ring).reshape(fs_count * share, width)
    gain_rows = norm_gain[None, :, None]
    rounded = (
        (expert_gate * gain_rows).astype(jnp.bfloat16),
        (expert_up * gain_rows).astype(jnp.bfloat16),
        expert_down.astype(jnp.bfloat16),
    )
    sample_gate, sample_up, sample_down = (
        lax.all_to_all(rounded[0], "fs", split_axis=0, concat_axis=1, tiled=True),
        lax.all_to_all(rounded[1], "fs", split_axis=0, concat_axis=1, tiled=True),
        lax.all_to_all(rounded[2], "fs", split_axis=0, concat_axis=1, tiled=True),
    )
    half = shared_gate.shape[1]
    shared_rows = jnp.concatenate(
        [
            (shared_gate * norm_gain[:, None]).astype(jnp.bfloat16),
            (shared_up * norm_gain[:, None]).astype(jnp.bfloat16),
            shared_down.astype(jnp.bfloat16),
        ],
        axis=1,
    )
    common = lax.all_gather(shared_rows, "fs", axis=0, tiled=False, axis_index_groups=groups)
    common_gate, common_up, common_down = (
        reorder(common[:, :, i * half : (i + 1) * half], place_of).reshape(width, half)
        for i in range(3)
    )
    shared_gate_act = jnp.dot(normed, common_gate, preferred_element_type=jnp.float32)
    shared_up_act = jnp.dot(normed, common_up, preferred_element_type=jnp.float32)
    shared_hidden = (jax.nn.silu(shared_gate_act) * shared_up_act).astype(jnp.bfloat16)
    shared_part = jnp.einsum(
        "th,dh->td", shared_hidden, common_down, preferred_element_type=jnp.float32
    ).astype(jnp.bfloat16)
    shared_parts = lax.all_to_all(
        shared_part.reshape(tok_rows, tp_count, width // tp_count).transpose(1, 0, 2),
        "tp",
        split_axis=0,
        concat_axis=0,
        tiled=True,
    )
    shared_sum = jnp.sum(shared_parts.astype(jnp.float32), axis=0)
    scale_all = reorder(
        lax.dynamic_slice_in_dim(dense_all, lax.axis_index("fs") * own_experts, own_experts, 1),
        ring,
    )
    total = None
    for expert in range(own_experts):
        scale = scale_all[:, expert, :].reshape(-1)[:, None]
        for shift in range(tp_count):
            gate_w, up_w, down_w = (sample_gate[expert], sample_up[expert], sample_down[expert])
            if shift:
                pairs = [(i, (i + shift) % tp_count) for i in range(tp_count)]
                gate_w, up_w, down_w = (
                    lax.ppermute(gate_w, "tp", pairs),
                    lax.ppermute(up_w, "tp", pairs),
                    lax.ppermute(down_w, "tp", pairs),
                )
            gate = jnp.dot(gathered, gate_w, preferred_element_type=jnp.float32)
            upward = jnp.dot(gathered, up_w, preferred_element_type=jnp.float32)
            hidden = (jax.nn.silu(gate) * upward * scale).astype(jnp.bfloat16)
            part = jnp.einsum("rf,df->rd", hidden, down_w, preferred_element_type=jnp.float32)
            total = part if total is None else total + part
    routed = lax.psum_scatter(
        total.astype(jnp.bfloat16), "fs", scatter_dimension=0, tiled=True, axis_index_groups=groups
    )
    routed = lax.all_to_all(routed, "tp", split_axis=1, concat_axis=0, tiled=True)
    layer_output = (routed.astype(jnp.float32) + shared_sum).astype(jnp.bfloat16)
    return (layer_output, sample_gate, sample_up, sample_down, common_gate, common_up, common_down)


def solution(mesh):
    return jax.shard_map(
        body,
        mesh=mesh,
        in_specs=(
            P("fs", None),
            P("fs", None),
            P("fs", None),
            P("fs"),
            P(None, "fs", "tp"),
            P(None, "fs", "tp"),
            P(None, "fs", "tp"),
            P("fs", "tp"),
            P("fs", "tp"),
            P("fs", "tp"),
        ),
        out_specs=(
            P("fs", "tp"),
            P("fs", None, "tp"),
            P("fs", None, "tp"),
            P("fs", None, "tp"),
            P(None, "tp"),
            P(None, "tp"),
            P(None, "tp"),
        ),
        check_vma=False,
    )
```

profile of v0, /device:TPU:0, one launch (start us, length us, event | category | flops | bytes accessed | tf_op | source)
XLA Modules:
  0.0 481.2 jit_solution(11208492477389067535)
XLA Ops:
  8.6 43.1 %all-gather = f32[256,128]{1,0:T(8,128)S(1)} all-gather(f32[16,128]{1,0:T(8,128)S(1)} %select_reduce_fusion), channel_id=2, replica_groups=mesh['fs'=16,'tp'=2] {'fs'}, dimensions={0}, use_global_device_ids=true | all-gather | bytes 139264 | tf_op jit(solution)/shard_map/all_gather | solution.py:59
  51.7 1.5 fusion
  53.2 1.5 fusion.1
  55.5 6.1 %multiply_convert_fusion.2 = (bf16[16,128,512]{2,1,0:T(8,128)(2,1)}, bf16[16,128,512]{2,1,0:T(8,128)(2,1)S(1)}) fusion(f32[16,128,512]{2,1,0:T(8,128)} %param.15, f32[128]{0:T(128)S(1)} %copy-done.8, f32[16,128,512]{2,1,0:T(8,128)} %param.14), kind=kLoop, calls=%fused_computation.3 | loop fusion | flops 4194304 | bytes 12583424 | tf_op jit(solution)/shard_map/convert_element_type | solution.py:66
  61.7 78.2 %all_to_all.54 = bf16[16,128,512]{2,1,0:T(8,128)(2,1)S(1)} all-to-all(bf16[16,128,512]{2,1,0:T(8,128)(2,1)S(1)} %get-tuple-element.57), channel_id=1, replica_groups=mesh['fs'=16,'tp'=2] {'fs'}, dimensions={0} | all-to-all | bytes 4194304 | tf_op jit(solution)/shard_map/all_to_all | solution.py:70
  139.9 4.5 all-to-all-start.1
  144.4 3.8 convert_element_type.59
  148.2 68.6 %all-to-all-done.1 = bf16[16,128,512]{2,1,0:T(8,128)(2,1)} async-done(((bf16[16,128,512]{2,1,0:T(8,128)(2,1)}), bf16[16,128,512]{2,1,0:T(8,128)(2,1)}, u32[]{:S(2)}, u32[]{:S(2)}) %all-to-all-start.1) | async-done | bytes 2097184 | tf_op jit(solution)/shard_map/all_to_all | solution.py:71
  216.8 22.6 %all-to-all-start.2 = ((bf16[16,128,512]{2,1,0:T(8,128)(2,1)}), bf16[16,128,512]{2,1,0:T(8,128)(2,1)}, u32[]{:S(2)}, u32[]{:S(2)}) async-start(bf16[16,128,512]{2,1,0:T(8,128)(2,1)} %convert_element_type.59), calls=%async_computation.2 | async-start | bytes 4194304 | tf_op jit(solution)/shard_map/all_to_all | solution.py:72
  239.4 1.1 multiply_convert_fusion.6
  242.5 57.3 %all-to-all-done.2 = bf16[16,128,512]{2,1,0:T(8,128)(2,1)} async-done(((bf16[16,128,512]{2,1,0:T(8,128)(2,1)}), bf16[16,128,512]{2,1,0:T(8,128)(2,1)}, u32[]{:S(2)}, u32[]{:S(2)}) %all-to-all-start.2) | async-done | bytes 2097184 | tf_op jit(solution)/shard_map/all_to_all | solution.py:72
  300.9 1.2 fusion.19
  302.1 1.8 fusion.18
  304.0 1.1 fusion.17
  305.1 1.1 fusion.16
  307.7 6.0 %fusion.30 = f32[2048,512]{1,0:T(8,128)} fusion(bf16[2048,2048]{1,0:T(8,128)(2,1)S(1)} %bitcast.140, bf16[2048,512]{1,0:T(8,128)(2,1)S(1)} %bitcast.104), kind=kOutput, calls=%fused_computation.142 | convolution fusion | flops 4294967296 | bytes 14680064 | tf_op jit(solution)/shard_map/dot_general | solution.py:118
  313.7 7.6 %fusion.31 = f32[2048,512]{1,0:T(8,128)} fusion(bf16[2048,2048]{1,0:T(8,128)(2,1)S(1)} %bitcast.141, bf16[2048,512]{1,0:T(8,128)(2,1)} %collective-permute-done), kind=kOutput, calls=%fused_computation.143 | convolution fusion | flops 4294967296 | bytes 14680064 | tf_op jit(solution)/shard_map/dot_general | solution.py:118
  321.3 7.6 %fusion.32 = f32[2048,512]{1,0:T(8,128)} fusion(bf16[2048,2048]{1,0:T(8,128)(2,1)S(1)} %bitcast.142, bf16[2048,512]{1,0:T(8,128)(2,1)} %collective-permute-done.1), kind=kOutput, calls=%fused_computation.144 | convolution fusion | flops 4294967296 | bytes 14680064 | tf_op jit(solution)/shard_map/dot_general | solution.py:119
  328.9 16.7 %fusion.6 = f32[2048,2048]{1,0:T(8,128)} fusion(bf16[2048,512]{1,0:T(8,128)(2,1)} %bitcast.20, f32[2048,512]{1,0:T(8,128)} %fusion.30, bf16[2048,2048]{1,0:T(8,128)(2,1)} %bitcast.143, bf16[2048,512]{1,0:T(8,128)(2,1)} %bitcast.18, f32[2048]{0:T(1024)S(1)} %bitcast.150), kind=kOutput, calls=%fused_computation.18 | convolution fusion | flops 8597274624 | bytes 33562624 | tf_op jit(solution)/shard_map/rf,df->rd/dot_general | solution.py:121
  345.6 13.5 %add_convert_fusion = bf16[2048,2048]{1,0:T(8,128)(2,1)} fusion(f32[2048,2048]{1,0:T(8,128)} %fusion.6, bf16[2048,512]{1,0:T(8,128)(2,1)} %collective-permute-done.2, f32[2048,512]{1,0:T(8,128)} %fusion.32, f32[2048,512]{1,0:T(8,128)} %fusion.31, f32[2048]{0:T(1024)S(1)} %bitcast.151), kind=kOutput, calls=%fused_computation | convolution fusion | flops 4310695936 | bytes 35659776 | tf_op jit(solution)/shard_map/rf,df->rd/dot_general | solution.py:121
  371.9 1.2 slice_dynamic-update-slice_fusion.2
  373.1 1.2 constant_dynamic-update-slice_fusion.17
  375.4 1.3 copy-done.5
  376.7 1.5 fusion.33
  378.2 4.8 convolution_convert_fusion
  383.0 1.3 copy.30
  384.3 4.6 all_to_all.55
  389.1 71.9 %reduce-scatter.2.cloned.1.call-done = bf16[128,2048]{1,0:T(8,128)(2,1)} async-done(((bf16[2048,2048]{1,0:T(8,128)(2,1)}), bf16[128,2048]{1,0:T(8,128)(2,1)}) %reduce-scatter.2.cloned.1.call-update) | async-done | bytes 524304 | tf_op jit(solution)/shard_map/reduce_scatter | solution.py:123
  462.1 4.2 all_to_all.56
  467.2 1.3 copy.105
  468.5 3.1 copy.106
  471.6 3.0 copy.107
  (82 shorter events, 22.9 us)
Async XLA Ops:
  7.2 0.7 copy-start
  7.2 292.6 %all-gather.6.cloned.1.call-start = ((), (), s32[]{:S(2)}) async-start(), calls=%async_computation.7 | async-start | bytes 8912896 | tf_op jit(solution)/shard_map/all_gather | solution.py:61
  53.2 2.4 copy-start.8
  139.9 76.9 %all-to-all-start.1 = ((bf16[16,128,512]{2,1,0:T(8,128)(2,1)}), bf16[16,128,512]{2,1,0:T(8,128)(2,1)}, u32[]{:S(2)}, u32[]{:S(2)}) async-start(bf16[16,128,512]{2,1,0:T(8,128)(2,1)} %get-tuple-element.56), calls=%async_computation.1 | async-start | bytes 4194304 | tf_op jit(solution)/shard_map/all_to_all | solution.py:71
  148.2 91.2 %copy-start.3 = (f32[128,512]{1,0:T(8,128)S(1)}, f32[128,512]{1,0:T(8,128)}, u32[]{:S(2)}) copy-start(f32[128,512]{1,0:T(8,128)} %param.19) | copy-start | bytes 786436
  216.8 83.0 %all-to-all-start.2 = ((bf16[16,128,512]{2,1,0:T(8,128)(2,1)}), bf16[16,128,512]{2,1,0:T(8,128)(2,1)}, u32[]{:S(2)}, u32[]{:S(2)}) async-start(bf16[16,128,512]{2,1,0:T(8,128)(2,1)} %convert_element_type.59), calls=%async_computation.2 | async-start | bytes 4194304 | tf_op jit(solution)/shard_map/all_to_all | solution.py:72
  239.4 119.8 %all-gather.8.cloned.1.call-start = ((), (), s32[]{:S(2)}) async-start(), calls=%async_computation.8 | async-start | bytes 6684672 | tf_op jit(solution)/shard_map/all_gather | solution.py:83
  241.4 219.7 %reduce-scatter.2.cloned.1.call-start = ((), (), s32[]{:S(2)}) async-start(), calls=%async_computation.6 | async-start | bytes 8912896 | tf_op jit(solution)/shard_map/reduce_scatter | solution.py:123
  241.9 71.8 %collective-permute-start = (bf16[2048,512]{1,0:T(8,128)(2,1)S(1)}, bf16[2048,512]{1,0:T(8,128)(2,1)}, u32[]{:S(2)}, u32[]{:S(2)}) collective-permute-start(bf16[2048,512]{1,0:T(8,128)(2,1)S(1)} %bitcast.103), channel_id=1, source_target_pairs={{0,1},{1,0},{2,3},{3,2},{4,5},{5,4},{6,7},{7,6},{8,9},{9,8},{10,11... | collective-permute-start | bytes 6291464 | tf_op jit(solution)/shard_map/ppermute | solution.py:114
  242.0 79.3 %collective-permute-start.1 = (bf16[2048,512]{1,0:T(8,128)(2,1)}, bf16[2048,512]{1,0:T(8,128)(2,1)}, u32[]{:S(2)}, u32[]{:S(2)}) collective-permute-start(bf16[2048,512]{1,0:T(8,128)(2,1)} %bitcast.18), channel_id=1, source_target_pairs={{0,1},{1,0},{2,3},{3,2},{4,5},{5,4},{6,7},{7,6},{8,9},{9,8},{10,11... | collective-permute-start | bytes 6291464 | tf_op jit(solution)/shard_map/ppermute | solution.py:115
  299.8 45.8 %collective-permute-start.2 = (bf16[2048,512]{1,0:T(8,128)(2,1)}, bf16[2048,512]{1,0:T(8,128)(2,1)}, u32[]{:S(2)}, u32[]{:S(2)}) collective-permute-start(bf16[2048,512]{1,0:T(8,128)(2,1)} %bitcast.20), channel_id=1, source_target_pairs={{0,1},{1,0},{2,3},{3,2},{4,5},{5,4},{6,7},{7,6},{8,9},{9,8},{10,11... | collective-permute-start | bytes 6291464 | tf_op jit(solution)/shard_map/ppermute | solution.py:116
  300.8 3.1 slice-start
  300.8 6.4 %copy-start.2 = (bf16[2048,2048]{1,0:T(8,128)(2,1)S(1)}, bf16[2048,2048]{1,0:T(8,128)(2,1)}, u32[]{:S(2)}) copy-start(bf16[2048,2048]{1,0:T(8,128)(2,1)} %all-gather.6.cloned.1.call-done) | copy-start | bytes 25165828
  307.7 13.6 %copy-start.4 = (bf16[16,128,2048]{2,1,0:T(8,128)(2,1)}, bf16[16,128,2048]{2,1,0:T(8,128)(2,1)S(1)}, u32[]{:S(2)}) copy-start(bf16[16,128,2048]{2,1,0:T(8,128)(2,1)S(1)} %fusion.7) | copy-start | bytes 25165828
  375.4 1.3 copy-start.5
  375.4 2.8 copy-start.6
  375.4 2.8 copy-start.7
  468.5 6.1 %copy-start.1 = (f32[256,6]{0,1:T(8,128)S(1)}, f32[256,6]{0,1:T(8,128)}, u32[]{:S(2)}) copy-start(f32[256,6]{0,1:T(8,128)} %param.12) | copy-start | bytes 18436
Sparse Core Ops, SparseCore 0:
  55.7 179.2 all-gather.5
  242.3 108.1 all-gather.7
  359.2 101.7 reduce-scatter.1
where the time goes:
time: 482 us; the launch traced here: 481 us
  waiting for transfers between devices  198 us (41%)
  blocking collectives  130 us (27%)
  matrix products  57.7 us (12%)
  local copies, waits for them, and re-layouts  37.5 us (8%)
  starting transfers between devices  27.9 us (6%)
  other arithmetic  16 us (3%)
  between operations  14.1 us (3%)
    all_to_all x1, blocking collectives, body(): lax.all_to_all(rounded[0], 'fs', split_axis=0, concat_axis=1, tiled=True)  78.2 us
    reduce_scatter x1, waiting for transfers between devices, body(): lax.psum_scatter(total.astype(jnp.bfloat16), 'fs', scatter_dimension=0, t...  71.9 us
    all_to_all x1, waiting for transfers between devices, body(): lax.all_to_all(rounded[1], 'fs', split_axis=0, concat_axis=1, tiled=True)  68.6 us
    all_to_all x1, waiting for transfers between devices, body(): lax.all_to_all(rounded[2], 'fs', split_axis=0, concat_axis=1, tiled=True)  57.3 us
    all_gather x1, blocking collectives, body(): dense_all = lax.all_gather(dense, 'fs', axis=0, tiled=False)  43.1 us
    unnamed x63, local copies, waits for them, and re-layouts  32.5 us
    dot_general x2, matrix products, body(): jnp.einsum('rf,df->rd', hidden, down_w, preferred_element_type=jnp.float32)  30.2 us
    all_to_all x1, starting transfers between devices, body(): lax.all_to_all(rounded[2], 'fs', split_axis=0, concat_axis=1, tiled=True)  22.6 us
  transfers between devices with their start and end apart: 8, of which 3 were waited for; matrix products, arithmetic and copies ran while one was open for 20% of the time, Pallas kernels for 0%

commit v1 on v0

--- a/solution.py
+++ b/solution.py
@@ -2,6 +2,7 @@
 import jax.numpy as jnp
 from jax import lax
 from jax.sharding import PartitionSpec as P
+from jax.lax import all_to_all, psum
 
 EPSILON = 1e-06
 
@@ -68,7 +69,10 @@
     )
     sample_gate, sample_up, sample_down = (
         lax.all_to_all(rounded[0], "fs", split_axis=0, concat_axis=1, tiled=True),
-        lax.all_to_all(rounded[1], "fs", split_axis=0, concat_axis=1, tiled=True),
+        jnp.concatenate(
+            all_to_all(jnp.stack(jnp.split(rounded[1], psum(1, "fs"), axis=0), axis=0), "fs", 0, 0),
+            axis=1,
+        ),
         lax.all_to_all(rounded[2], "fs", split_axis=0, concat_axis=1, tiled=True),
     )
     half = shared_gate.shape[1]

time: 482 us -> 487 us (1.010)
  blocking collectives: 130 us -> 51.9 us
  waiting for transfers between devices: 198 us -> 251 us
  starting transfers between devices: 27.9 us -> 44.2 us
  local copies, waits for them, and re-layouts: 37.5 us -> 48.1 us
    all_to_all x1 -> x0, blocking collectives: 78.2 us -> none  [body(): lax.all_to_all(rounded[0], 'fs', split_axis=0, concat_axis=1, tiled=True)]
    all_to_all x1 -> x2, waiting for transfers between devices: 68.6 us -> 123 us  [the longest x1 68.5 us: body(): all_to_all(jnp.stack(jnp.split(rounded[1], psum(1, 'fs'), axis=0), axis=0...]
    all_to_all x1 -> x2, starting transfers between devices: 4.49 us -> 19.3 us  [the longest x1 14.9 us: body(): all_to_all(jnp.stack(jnp.split(rounded[1], psum(1, 'fs'), axis=0), axis=0...]
    unnamed x63 -> x78, local copies, waits for them, and re-layouts: 32.5 us -> 42.4 us
  transfers between devices with their start and end apart: 8 -> 9, of which waited for: 3 -> 4; matrix products, arithmetic and copies ran while one was open for 20% -> 22% of each run, Pallas kernels for 0% -> 0%
where the time goes in v1:
time: 487 us; the launch traced here: 486 us
  waiting for transfers between devices  251 us (52%)
  matrix products  60.2 us (12%)
  blocking collectives  51.9 us (11%)
  local copies, waits for them, and re-layouts  48.1 us (10%)
  starting transfers between devices  44.2 us (9%)
  other arithmetic  16.3 us (3%)
  between operations  14.1 us (3%)
    reduce_scatter x1, waiting for transfers between devices, body(): lax.psum_scatter(total.astype(jnp.bfloat16), 'fs', scatter_dimension=0, t...  71.6 us
    all_to_all x1, waiting for transfers between devices, body(): all_to_all(jnp.stack(jnp.split(rounded[1], psum(1, 'fs'), axis=0), axis=0...  68.5 us
    all_to_all x1, waiting for transfers between devices, body(): lax.all_to_all(rounded[2], 'fs', split_axis=0, concat_axis=1, tiled=True)  56.9 us
    all_to_all x1, waiting for transfers between devices, body(): lax.all_to_all(rounded[0], 'fs', split_axis=0, concat_axis=1, tiled=True)  54.2 us
    all_gather x1, blocking collectives, body(): dense_all = lax.all_gather(dense, 'fs', axis=0, tiled=False)  43.1 us
    unnamed x78, local copies, waits for them, and re-layouts  42.4 us
    dot_general x2, matrix products, body(): jnp.einsum('rf,df->rd', hidden, down_w, preferred_element_type=jnp.float32)  29.6 us
    all_to_all x1, starting transfers between devices, body(): lax.all_to_all(rounded[2], 'fs', split_axis=0, concat_axis=1, tiled=True)  24 us
  transfers between devices with their start and end apart: 9, of which 4 were waited for; matrix products, arithmetic and copies ran while one was open for 22% of the time, Pallas kernels for 0%

profile of v1, /device:TPU:0, one launch (start us, length us, event | category | flops | bytes accessed | tf_op | source)
XLA Modules:
  0.0 486.1 jit_solution(1355189986930438486)
XLA Ops:
  8.6 43.1 %all-gather = f32[256,128]{1,0:T(8,128)S(1)} all-gather(f32[16,128]{1,0:T(8,128)S(1)} %select_reduce_fusion), channel_id=2, replica_groups=mesh['fs'=16,'tp'=2] {'fs'}, dimensions={0}, use_global_device_ids=true | all-gather | bytes 139264 | tf_op jit(solution)/shard_map/all_gather | solution.py:60
  51.7 1.5 fusion
  53.2 1.5 fusion.1
  55.5 6.1 %multiply_convert_fusion.2 = (bf16[16,128,512]{2,1,0:T(8,128)(2,1)S(1)}, bf16[16,128,512]{2,1,0:T(8,128)(2,1)}) fusion(f32[16,128,512]{2,1,0:T(8,128)} %param.15, f32[128]{0:T(128)S(1)} %copy-done.8, f32[16,128,512]{2,1,0:T(8,128)} %param.14), kind=kLoop, calls=%fused_computation.3 | loop fusion | flops 4194304 | bytes 12583424 | tf_op jit(solution)/shard_map/convert_element_type | solution.py:67
  61.7 4.4 all-to-all-start
  76.7 54.2 %all-to-all-done = bf16[16,128,512]{2,1,0:T(8,128)(2,1)} async-done(((bf16[16,128,512]{2,1,0:T(8,128)(2,1)}), bf16[16,128,512]{2,1,0:T(8,128)(2,1)}, u32[]{:S(2)}, u32[]{:S(2)}) %all-to-all-start) | async-done | bytes 2097184 | tf_op jit(solution)/shard_map/all_to_all | solution.py:71
  130.9 14.9 %all-to-all-start.1 = ((bf16[16,1,128,512]{3,2,1,0:T(8,128)(2,1)}), bf16[16,1,128,512]{3,2,1,0:T(8,128)(2,1)S(1)}, u32[]{:S(2)}, u32[]{:S(2)}) async-start(bf16[16,1,128,512]{3,2,1,0:T(8,128)(2,1)} %constant_dynamic-update-slice_fusion.1), calls=%async_computation.1 | async-start | bytes 4194304 | tf_op jit(solution)/shard_map/all_to_all | solution.py:73
  145.8 4.1 convert_element_type.59
  149.9 68.5 %all-to-all-done.1 = bf16[16,1,128,512]{3,2,1,0:T(8,128)(2,1)S(1)} async-done(((bf16[16,1,128,512]{3,2,1,0:T(8,128)(2,1)}), bf16[16,1,128,512]{3,2,1,0:T(8,128)(2,1)S(1)}, u32[]{:S(2)}, u32[]{:S(2)}) %all-to-all-start.1) | async-done | bytes 2097184 | tf_op jit(solution)/shard_map/all_to_all | solution.py:73
  218.4 24.0 %all-to-all-start.2 = ((bf16[16,128,512]{2,1,0:T(8,128)(2,1)}), bf16[16,128,512]{2,1,0:T(8,128)(2,1)}, u32[]{:S(2)}, u32[]{:S(2)}) async-start(bf16[16,128,512]{2,1,0:T(8,128)(2,1)} %convert_element_type.59), calls=%async_computation.2 | async-start | bytes 4194304 | tf_op jit(solution)/shard_map/all_to_all | solution.py:76
  242.5 1.1 multiply_convert_fusion.6
  245.6 56.9 %all-to-all-done.2 = bf16[16,128,512]{2,1,0:T(8,128)(2,1)} async-done(((bf16[16,128,512]{2,1,0:T(8,128)(2,1)}), bf16[16,128,512]{2,1,0:T(8,128)(2,1)}, u32[]{:S(2)}, u32[]{:S(2)}) %all-to-all-start.2) | async-done | bytes 2097184 | tf_op jit(solution)/shard_map/all_to_all | solution.py:76
  303.6 1.2 fusion.19
  304.8 1.8 fusion.18
  307.8 1.1 fusion.16
  310.4 9.2 %fusion.30 = f32[2048,512]{1,0:T(8,128)} fusion(bf16[2048,2048]{1,0:T(8,128)(2,1)S(1)} %bitcast.204, bf16[2048,512]{1,0:T(8,128)(2,1)} %bitcast.17), kind=kOutput, calls=%fused_computation.174 | convolution fusion | flops 4294967296 | bytes 14680064 | tf_op jit(solution)/shard_map/dot_general | solution.py:122
  319.6 7.5 %fusion.32 = f32[2048,512]{1,0:T(8,128)} fusion(bf16[2048,2048]{1,0:T(8,128)(2,1)S(1)} %bitcast.205, bf16[2048,512]{1,0:T(8,128)(2,1)} %collective-permute-done.1), kind=kOutput, calls=%fused_computation.176 | convolution fusion | flops 4294967296 | bytes 14680064 | tf_op jit(solution)/shard_map/dot_general | solution.py:123
  327.2 7.6 %fusion.31 = f32[2048,512]{1,0:T(8,128)} fusion(bf16[2048,2048]{1,0:T(8,128)(2,1)S(1)} %bitcast.206, bf16[2048,512]{1,0:T(8,128)(2,1)} %collective-permute-done), kind=kOutput, calls=%fused_computation.175 | convolution fusion | flops 4294967296 | bytes 14680064 | tf_op jit(solution)/shard_map/dot_general | solution.py:122
  334.8 16.1 %fusion.6 = f32[2048,2048]{1,0:T(8,128)} fusion(bf16[2048,512]{1,0:T(8,128)(2,1)} %bitcast.36, f32[2048,512]{1,0:T(8,128)} %fusion.30, bf16[2048,2048]{1,0:T(8,128)(2,1)} %bitcast.207, bf16[2048,512]{1,0:T(8,128)(2,1)S(1)} %bitcast.168, f32[2048]{0:T(1024)S(1)} %bitcast.214), kind=kOutput, calls=%fused_computation.18 | convolution fusion | flops 8597274624 | bytes 33562624 | tf_op jit(solution)/shard_map/rf,df->rd/dot_general | solution.py:125
  350.9 13.5 %add_convert_fusion = bf16[2048,2048]{1,0:T(8,128)(2,1)} fusion(f32[2048,2048]{1,0:T(8,128)} %fusion.6, bf16[2048,512]{1,0:T(8,128)(2,1)} %collective-permute-done.2, f32[2048,512]{1,0:T(8,128)} %fusion.32, f32[2048,512]{1,0:T(8,128)} %fusion.31, f32[2048]{0:T(1024)S(1)} %bitcast.215), kind=kOutput, calls=%fused_computation | convolution fusion | flops 4310695936 | bytes 35659776 | tf_op jit(solution)/shard_map/rf,df->rd/dot_general | solution.py:125
  377.2 1.2 slice_dynamic-update-slice_fusion.2
  378.4 1.1 constant_dynamic-update-slice_fusion.33
  380.6 1.3 copy-done.5
  381.9 1.5 fusion.33
  383.4 4.8 convolution_convert_fusion
  388.1 1.3 copy.30
  389.5 4.7 all_to_all.47
  394.3 71.6 %reduce-scatter.2.cloned.1.call-done = bf16[128,2048]{1,0:T(8,128)(2,1)} async-done(((bf16[2048,2048]{1,0:T(8,128)(2,1)}), bf16[128,2048]{1,0:T(8,128)(2,1)}) %reduce-scatter.2.cloned.1.call-update) | async-done | bytes 524304 | tf_op jit(solution)/shard_map/reduce_scatter | solution.py:127
  467.0 4.2 all_to_all.48
  472.1 3.0 copy.120
  475.2 1.3 copy.121
  476.5 3.0 copy.122
  (99 shorter events, 34.6 us)
Async XLA Ops:
  7.2 0.7 copy-start
  7.2 295.3 %all-gather.6.cloned.1.call-start = ((), (), s32[]{:S(2)}) async-start(), calls=%async_computation.7 | async-start | bytes 8912896 | tf_op jit(solution)/shard_map/all_gather | solution.py:62
  53.2 2.4 copy-start.8
  61.7 69.2 %all-to-all-start = ((bf16[16,128,512]{2,1,0:T(8,128)(2,1)}), bf16[16,128,512]{2,1,0:T(8,128)(2,1)}, u32[]{:S(2)}, u32[]{:S(2)}) async-start(bf16[16,128,512]{2,1,0:T(8,128)(2,1)} %get-tuple-element.57), calls=%async_computation | async-start | bytes 4194304 | tf_op jit(solution)/shard_map/all_to_all | solution.py:71
  130.9 87.5 %all-to-all-start.1 = ((bf16[16,1,128,512]{3,2,1,0:T(8,128)(2,1)}), bf16[16,1,128,512]{3,2,1,0:T(8,128)(2,1)S(1)}, u32[]{:S(2)}, u32[]{:S(2)}) async-start(bf16[16,1,128,512]{3,2,1,0:T(8,128)(2,1)} %constant_dynamic-update-slice_fusion.1), calls=%async_computation.1 | async-start | bytes 4194304 | tf_op jit(solution)/shard_map/all_to_all | solution.py:73
  149.9 92.6 %copy-start.3 = (f32[128,512]{1,0:T(8,128)S(1)}, f32[128,512]{1,0:T(8,128)}, u32[]{:S(2)}) copy-start(f32[128,512]{1,0:T(8,128)} %param.19) | copy-start | bytes 786436
  218.4 84.1 %all-to-all-start.2 = ((bf16[16,128,512]{2,1,0:T(8,128)(2,1)}), bf16[16,128,512]{2,1,0:T(8,128)(2,1)}, u32[]{:S(2)}, u32[]{:S(2)}) async-start(bf16[16,128,512]{2,1,0:T(8,128)(2,1)} %convert_element_type.59), calls=%async_computation.2 | async-start | bytes 4194304 | tf_op jit(solution)/shard_map/all_to_all | solution.py:76
  242.4 122.0 %all-gather.8.cloned.1.call-start = ((), (), s32[]{:S(2)}) async-start(), calls=%async_computation.8 | async-start | bytes 6684672 | tf_op jit(solution)/shard_map/all_gather | solution.py:87
  244.4 221.5 %reduce-scatter.2.cloned.1.call-start = ((), (), s32[]{:S(2)}) async-start(), calls=%async_computation.6 | async-start | bytes 8912896 | tf_op jit(solution)/shard_map/reduce_scatter | solution.py:127
  245.0 74.6 %collective-permute-start.1 = (bf16[2048,512]{1,0:T(8,128)(2,1)S(1)}, bf16[2048,512]{1,0:T(8,128)(2,1)}, u32[]{:S(2)}, u32[]{:S(2)}) collective-permute-start(bf16[2048,512]{1,0:T(8,128)(2,1)S(1)} %bitcast.167), channel_id=1, source_target_pairs={{0,1},{1,0},{2,3},{3,2},{4,5},{5,4},{6,7},{7,6},{8,9},{9,8},{10,11... | collective-permute-start | bytes 6291464 | tf_op jit(solution)/shard_map/ppermute | solution.py:119
  245.1 82.1 %collective-permute-start = (bf16[2048,512]{1,0:T(8,128)(2,1)}, bf16[2048,512]{1,0:T(8,128)(2,1)}, u32[]{:S(2)}, u32[]{:S(2)}) collective-permute-start(bf16[2048,512]{1,0:T(8,128)(2,1)} %bitcast.17), channel_id=1, source_target_pairs={{0,1},{1,0},{2,3},{3,2},{4,5},{5,4},{6,7},{7,6},{8,9},{9,8},{10,11... | collective-permute-start | bytes 6291464 | tf_op jit(solution)/shard_map/ppermute | solution.py:118
  302.5 48.4 %collective-permute-start.2 = (bf16[2048,512]{1,0:T(8,128)(2,1)}, bf16[2048,512]{1,0:T(8,128)(2,1)}, u32[]{:S(2)}, u32[]{:S(2)}) collective-permute-start(bf16[2048,512]{1,0:T(8,128)(2,1)} %bitcast.36), channel_id=1, source_target_pairs={{0,1},{1,0},{2,3},{3,2},{4,5},{5,4},{6,7},{7,6},{8,9},{9,8},{10,11... | collective-permute-start | bytes 6291464 | tf_op jit(solution)/shard_map/ppermute | solution.py:120
  303.5 3.1 slice-start
  303.6 6.4 %copy-start.2 = (bf16[2048,2048]{1,0:T(8,128)(2,1)S(1)}, bf16[2048,2048]{1,0:T(8,128)(2,1)}, u32[]{:S(2)}) copy-start(bf16[2048,2048]{1,0:T(8,128)(2,1)} %all-gather.6.cloned.1.call-done) | copy-start | bytes 25165828
  310.4 16.8 %copy-start.4 = (bf16[16,128,2048]{2,1,0:T(8,128)(2,1)}, bf16[16,128,2048]{2,1,0:T(8,128)(2,1)S(1)}, u32[]{:S(2)}) copy-start(bf16[16,128,2048]{2,1,0:T(8,128)(2,1)S(1)} %fusion.7) | copy-start | bytes 25165828
  380.5 1.3 copy-start.5
  380.6 2.8 copy-start.6
  380.6 2.8 copy-start.7
  475.2 4.4 copy-start.1
Sparse Core Ops, SparseCore 0:
  55.7 182.6 all-gather.5
  245.3 107.7 all-gather.7
  364.5 101.4 reduce-scatter.1
